TPU v7x, 32 devices: a whole 2x2x4 slice. The times are simulated.
32 devices in a mesh: sp: 4 (over z), fs: 4 (over y, x), tp: 2 (over core).
Axes of the slice: x: 2, y: 2, z: 4, core: 2. Of those that a mesh axis runs over, the one named last changes fastest.
Arguments:
- tokens: bfloat16 [4096, 2048], P(('fs', 'sp')), parts along dimension 0, may hold values from -6 to 6
- norm_gain: float32 [2048], replicated, may hold values from 0.1 to 1.9
- w_query: bfloat16 [2048, 1024], P('sp', 'tp'), may hold values from -0.080939698 to 0.080939698
- w_key: bfloat16 [2048, 256], P('sp', 'tp'), may hold values from -0.080939698 to 0.080939698
- w_value: bfloat16 [2048, 256], P('sp', 'tp'), may hold values from -0.125 to 0.125
- w_conv_in: bfloat16 [2048, 1024], P('sp', 'tp'), may hold values from -0.125 to 0.125
- w_conv_gate: bfloat16 [2048, 1024], P('sp', 'tp'), may hold values from -0.125 to 0.125
- sink_logit: float32 [16], P('tp'), may hold values from 2 to 6
- conv_taps: float32 [31, 1024], P(None, 'tp'), may hold values from -5.3881591 to 5.3881591
- conv_bias: float32 [1024], P('tp'), may hold values from -0.9 to 5.9
- channel_gain: float32 [1024], P('tp'), may hold values from 0.1 to 1.9
- channel_shift: float32 [1024], P('tp'), may hold values from -3 to 3
- w_attn_out: bfloat16 [1024, 2048], P(None, 'sp'), may hold values from -1.5 to 1.5
- w_conv_out: bfloat16 [1024, 2048], P(None, 'sp'), may hold values from -0.1875 to 0.1875
Outputs:
- output: bfloat16 [4096, 2048], P(('fs', 'sp', 'tp')), parts along dimension 0
There are 4 independent parts, one for each index of `fs`. A program takes and returns all parts, laid end to end along the dimension named above; an argument that names none is the same for every part. Nothing has to cross between parts.
All inputs are finite; a program needn't handle non-finite values.
Results may differ from a plain program's by a relative error of at most 0.011.
Values may be sent and summed in bfloat16 or wider, within the bound.
A program may use at most 64 MiB of HBM per device.

v0:
```python
import jax
import jax.numpy as jnp
from jax import lax
from jax.sharding import PartitionSpec as P

HEAD_DIM = 64
WINDOW = 128
GRID_W = 64
EPSILON = 1e-06
NEGATIVE = -1e30
ROPE_BASE = 10000.0


def padded(block, sides, width):
    for axis, dim in sides:
        count = lax.axis_size(axis)
        forward = [(i, i + 1) for i in range(count - 1)]
        backward = [(target, source) for source, target in forward]
        low = lax.ppermute(
            lax.slice_in_dim(block, block.shape[dim] - width, None, axis=dim), axis, forward
        )
        high = lax.ppermute(lax.slice_in_dim(block, 0, width, axis=dim), axis, backward)
        block = jnp.concatenate([low, block, high], axis=dim)
    return block


def rotate_pairs(values, positions):
    middle = values.shape[-1] // 2
    inverse = ROPE_BASE ** (-jnp.arange(middle, dtype=jnp.float32) / middle)
    angles = positions.astype(jnp.float32)[:, None] * inverse[None, :]
    cosine = jnp.cos(angles)[:, None, :]
    sine_table = jnp.sin(angles)[:, None, :]
    leading = values[..., :middle]
    trailing = values[..., middle:]
    return jnp.concatenate(
        [leading * cosine - trailing * sine_table, leading * sine_table + trailing * cosine],
        axis=-1,
    )


def grid_rotate(values, positions):
    middle = values.shape[-1] // 2
    return jnp.concatenate(
        [
            rotate_pairs(values[..., :middle], positions // GRID_W),
            rotate_pairs(values[..., middle:], positions % GRID_W),
        ],
        axis=-1,
    )


def local(
    tokens,
    norm_gain,
    w_query,
    w_key,
    w_value,
    w_conv_in,
    w_conv_gate,
    sink_logit,
    conv_taps,
    conv_bias,
    channel_gain,
    channel_shift,
    w_attn_out,
    w_conv_out,
):
    rows_here = tokens.shape[0]
    offset = lax.axis_index("sp") * rows_here
    total = rows_here * lax.axis_size("sp")
    tp_count = lax.axis_size("tp")
    token_float = tokens.astype(jnp.float32)
    normed = (
        token_float
        * lax.rsqrt(jnp.mean(token_float * token_float, axis=-1, keepdims=True) + EPSILON)
        * norm_gain[None, :]
    ).astype(jnp.bfloat16)
    head_cols = w_query.shape[1]
    kv_cols = w_key.shape[1]
    chan_cols = w_conv_in.shape[1]
    piece_query = lax.all_gather(w_query, "sp", axis=0, tiled=True)
    piece_key = lax.all_gather(w_key, "sp", axis=0, tiled=True)
    piece_value = lax.all_gather(w_value, "sp", axis=0, tiled=True)
    piece_conv = lax.all_gather(w_conv_in, "sp", axis=0, tiled=True)
    piece_gate = lax.all_gather(w_conv_gate, "sp", axis=0, tiled=True)
    query_acc = jnp.dot(normed, piece_query, preferred_element_type=jnp.float32)
    pair_acc = jnp.dot(
        normed,
        jnp.concatenate([piece_key, piece_value], axis=1),
        preferred_element_type=jnp.float32,
    )
    conv_acc = jnp.dot(
        normed,
        jnp.concatenate([piece_conv, piece_gate], axis=1),
        preferred_element_type=jnp.float32,
    )
    positions = offset + jnp.arange(rows_here, dtype=jnp.int32)
    heads_here = head_cols // HEAD_DIM
    kv_here = kv_cols // HEAD_DIM
    group = heads_here // kv_here
    query = grid_rotate(query_acc.reshape(rows_here, heads_here, HEAD_DIM), positions).astype(
        jnp.bfloat16
    )
    keys = grid_rotate(pair_acc[:, :kv_cols].reshape(rows_here, kv_here, HEAD_DIM), positions)
    keys = keys.astype(jnp.bfloat16).reshape(rows_here, kv_cols)
    values = pair_acc[:, kv_cols:].astype(jnp.bfloat16)
    stacked = jnp.concatenate([keys, values], axis=1)
    extended = padded(stacked, (("sp", 0),), WINDOW)
    block = min(rows_here, 512)
    span = block + 2 * WINDOW
    sinks = sink_logit.reshape(kv_here, group)[:, :, None, None]
    queries = query.reshape(block, kv_here, group, HEAD_DIM)
    near_keys = extended[:, :kv_cols].reshape(span, kv_here, HEAD_DIM)
    near_values = extended[:, kv_cols:].reshape(span, kv_here, HEAD_DIM)
    scores = jnp.einsum(
        "qkgd,skd->kgqs", queries, near_keys, preferred_element_type=jnp.float32
    ) * HEAD_DIM ** (-0.5)
    query_pos = offset + 0 + jnp.arange(block, dtype=jnp.int32)
    key_pos = offset + 0 - WINDOW + jnp.arange(span, dtype=jnp.int32)
    valid = (
        (jnp.abs(query_pos[:, None] - key_pos[None, :]) <= WINDOW)
        & (key_pos[None, :] >= 0)
        & (key_pos[None, :] < total)
    )
    scores = jnp.where(valid[None, None], scores, NEGATIVE)
    top = jnp.maximum(jnp.max(scores, axis=-1, keepdims=True), sinks)
    raised = jnp.exp(scores - top)
    denominator = jnp.sum(raised, axis=-1, keepdims=True) + jnp.exp(sinks - top)
    probs = (raised / denominator).astype(jnp.bfloat16)
    mixed = jnp.einsum("kgqs,skd->qkgd", probs, near_values, preferred_element_type=jnp.float32)
    outputs = mixed.astype(jnp.bfloat16).reshape(block, head_cols)
    glu = (conv_acc[:, :chan_cols] * jax.nn.sigmoid(conv_acc[:, chan_cols:])).astype(jnp.bfloat16)
    reach = conv_taps.shape[0] // 2
    rims = padded(glu, (("sp", 0),), reach)
    filtered = jnp.zeros((rows_here, chan_cols), jnp.float32) + conv_bias[None, :]
    for shift_index in range(conv_taps.shape[0]):
        filtered = filtered + conv_taps[shift_index][None, :] * rims[
            shift_index : shift_index + rows_here
        ].astype(jnp.float32)
    channel_total = chan_cols * tp_count
    centre = lax.psum(jnp.sum(filtered, axis=-1), "tp")[:, None] / channel_total
    centred = filtered - centre
    spread = lax.psum(jnp.sum(centred * centred, axis=-1), "tp")[:, None] / channel_total
    conv_out = jax.nn.silu(
        centred * lax.rsqrt(spread + EPSILON) * channel_gain[None, :] + channel_shift[None, :]
    ).astype(jnp.bfloat16)
    features = jnp.concatenate([outputs, conv_out], axis=1)
    tp_here = lax.axis_index("tp")
    own_rows = jnp.concatenate(
        [
            lax.dynamic_slice_in_dim(w_attn_out, tp_here * head_cols, head_cols, 0),
            lax.dynamic_slice_in_dim(w_conv_out, tp_here * chan_cols, chan_cols, 0),
        ],
        axis=0,
    )
    own_whole = lax.all_gather(own_rows, "sp", axis=1, tiled=True)
    result = lax.psum_scatter(
        jnp.dot(features, own_whole, preferred_element_type=jnp.float32).astype(jnp.bfloat16),
        "tp",
        scatter_dimension=0,
        tiled=True,
    )
    return result


def solution(mesh):
    in_specs = (
        P(("fs", "sp"), None),
        P(),
        P("sp", "tp"),
        P("sp", "tp"),
        P("sp", "tp"),
        P("sp", "tp"),
        P("sp", "tp"),
        P("tp"),
        P(None, "tp"),
        P("tp"),
        P("tp"),
        P("tp"),
        P(None, "sp"),
        P(None, "sp"),
    )
    out_specs = P(("fs", "sp", "tp"), None)
    return jax.shard_map(local, mesh=mesh, in_specs=in_specs, out_specs=out_specs, check_vma=False)
```

profile of v0, /device:TPU:0, one launch (start us, length us, event | category | flops | bytes accessed | tf_op | source)
XLA Modules:
  0.0 263.5 jit_solution(13735289390232705822)
XLA Ops:
  6.5 0.0 copy-start
  6.5 0.0 copy-start.1
  6.5 0.0 all-gather.7.cloned.1.call-start
  6.5 0.7 all-gather.7.cloned.1.call-update
  7.3 0.0 all-gather.9.cloned.1.call-start
  7.3 0.7 all-gather.9.cloned.1.call-update
  8.0 0.0 copy-start.7
  8.0 0.0 all-gather.5.cloned.1.call-start
  8.1 0.7 all-gather.5.cloned.1.call-update
  8.8 0.0 all-gather.11.cloned.1.call-start
  8.8 1.3 constant_dynamic-slice_fusion
  10.1 1.0 pad_maximum_fusion
  11.1 0.0 copy-start.3
  11.1 0.0 all-gather.11.cloned.1.call-update
  11.2 0.0 reduce-scatter.2.cloned.1.call-start
  11.3 0.0 copy-done
  11.3 0.3 fusion.6
  11.6 0.0 copy-done.1
  11.6 23.1 %all_gather.18 = bf16[2048,128]{1,0:T(8,128)(2,1)S(1)} all-gather(bf16[512,128]{1,0:T(8,128)(2,1)S(1)} %copy-done.1), channel_id=1, replica_groups=mesh['sp'=4,'fs'=4,'tp'=2] {'sp'}, dimensions={0}, use_global_device_ids=true | all-gather | bytes 655360 | tf_op jit(solution)/shard_map/all_gather | solution.py:82
  34.7 0.0 copy-done.2
  34.7 21.7 %all_gather.19 = bf16[2048,128]{1,0:T(8,128)(2,1)S(1)} all-gather(bf16[512,128]{1,0:T(8,128)(2,1)S(1)} %copy-done.2), channel_id=1, replica_groups=mesh['sp'=4,'fs'=4,'tp'=2] {'sp'}, dimensions={0}, use_global_device_ids=true | all-gather | bytes 655360 | tf_op jit(solution)/shard_map/all_gather | solution.py:83
  56.4 0.0 copy-done.7
  56.4 0.7 fusion.11
  57.1 0.2 multiply_cosine_fusion.1
  57.4 1.5 collective-permute-start
  58.9 1.3 collective-permute-start.1
  60.2 0.0 copy-done.3
  60.3 0.3 fusion.24
  60.6 0.0 copy-done.8
  60.6 0.1 max.18
  60.7 1.5 collective-permute-done
  62.2 7.0 %collective-permute-done.1 = bf16[128,256]{0,1:T(8,128)(2,1)S(1)} collective-permute-done((bf16[128,256]{0,1:T(8,128)(2,1)S(1)}, bf16[128,256]{0,1:T(8,128)(2,1)S(1)}, u32[]{:S(2)}, u32[]{:S(2)}) %collective-permute-start.1) | collective-permute-done | bytes 65568 | tf_op jit(solution)/shard_map/ppermute | solution.py:22
  69.2 1.9 all-gather.7.cloned.1.call-done
  71.1 47.3 %all-gather.9.cloned.1.call-done = bf16[2048,512]{1,0:T(8,128)(2,1)} async-done(((bf16[512,512]{1,0:T(8,128)(2,1)}), bf16[2048,512]{1,0:T(8,128)(2,1)}) %all-gather.9.cloned.1.call-update) | async-done | bytes 2097168 | tf_op jit(solution)/shard_map/all_gather | solution.py:85
  118.4 3.5 %fusion = f32[256,1024]{1,0:T(8,128)S(1)} fusion(bf16[2048,512]{1,0:T(8,128)(2,1)} %all-gather.9.cloned.1.call-done, bf16[2048,512]{1,0:T(8,128)(2,1)} %all-gather.7.cloned.1.call-done, bf16[256,2048]{1,0:T(8,128)(2,1)S(1)} %copy-done, f32[2048]{0:T(1024)S(1)} %copy-done.7, f32[256]{0:T(256)S(1)} %add_rsqrt_fusion.1), kind=kOutput, calls=%fused_computation | convolution fusion | flops 1084227584 | bytes 6300672 | tf_op jit(solution)/shard_map/dot_general | solution.py:92
  121.9 0.1 fusion.22
  122.1 2.1 collective-permute-start.2
  124.2 1.3 collective-permute-start.3
  125.5 39.2 %all-gather.5.cloned.1.call-done = bf16[2048,512]{1,0:T(8,128)(2,1)} async-done(((bf16[512,512]{1,0:T(8,128)(2,1)}), bf16[2048,512]{1,0:T(8,128)(2,1)}) %all-gather.5.cloned.1.call-update) | async-done | bytes 2097168 | tf_op jit(solution)/shard_map/all_gather | solution.py:81
  164.6 2.6 fusion.74
  167.2 0.1 subtract_convert_fusion.1
  167.3 0.8 fusion.5
  168.2 0.1 broadcast_maximum_fusion
  168.2 0.9 fusion.4
  169.1 0.1 exponential_add_fusion
  169.2 0.0 copy-start.4
  169.2 0.0 copy-start.5
  169.2 0.0 copy-start.6
  169.3 1.2 fusion.10
  170.5 0.1 copy.27
  170.6 0.0 collective-permute-done.2
  170.6 0.0 collective-permute-done.3
  170.7 0.0 copy-done.4
  170.7 3.1 %fusion.77 = (f32[256]{0:T(256)S(1)}, f32[256,512]{1,0:T(8,128)S(1)}) fusion(bf16[15,512]{1,0:T(8,128)(2,1)S(1)} %collective-permute-done.3, bf16[256,512]{1,0:T(8,128)(2,1)S(1)} %fusion.22, f32[512]{0:T(512)S(1)} %bitcast.106, f32[512]{0:T(512)S(1)} %bitcast.107, f32[512]{0:T(512)S(1)} %bitcast.78, f32[512]{0:T(512)S(1)} %bitcast.79, f32[512]{0:T(512)S(1)} %bitcast.80, ...), kind=kLoop, calls=%fused_computation.167 | loop fusion | flops 24116992 | bytes 883712 | tf_op jit(solution)/shard_map/reduce_sum | solution.py:141
  173.8 2.5 psum.14
  176.2 0.2 multiply_reduce_fusion
  176.4 2.5 psum.15
  178.9 0.0 copy-done.5
  178.9 0.0 copy-done.6
  178.9 0.3 multiply_convert_fusion
  179.2 66.3 %all-gather.11.cloned.1.call-done = bf16[1024,2048]{1,0:T(8,128)(2,1)} async-done(((bf16[1024,512]{1,0:T(8,128)(2,1)}), bf16[1024,2048]{1,0:T(8,128)(2,1)}) %all-gather.11.cloned.1.call-update) | async-done | bytes 4194320 | tf_op jit(solution)/shard_map/all_gather | solution.py:156
  245.5 4.5 %convolution_convert_fusion = bf16[256,2048]{1,0:T(8,128)(2,1)} fusion(bf16[1024,2048]{1,0:T(8,128)(2,1)} %all-gather.11.cloned.1.call-done, bf16[256,512]{1,0:T(8,128)(2,1)S(1)} %multiply_convert_fusion, bf16[256,512]{1,0:T(8,128)(2,1)S(1)} %copy.27), kind=kOutput, calls=%fused_computation.11 | convolution fusion | flops 1075314688 | bytes 5767168 | tf_op jit(solution)/shard_map/dot_general | solution.py:158
  249.9 0.0 reduce-scatter.2.cloned.1.call-update
  249.9 7.0 %reduce-scatter.2.cloned.1.call-done = bf16[128,2048]{1,0:T(8,128)(2,1)} async-done(((bf16[256,2048]{1,0:T(8,128)(2,1)}), bf16[128,2048]{1,0:T(8,128)(2,1)}) %reduce-scatter.2.cloned.1.call-update) | async-done | bytes 524304 | tf_op jit(solution)/shard_map/reduce_scatter | solution.py:157
  (20 shorter events, 0.3 us)
Async XLA Ops:
  6.5 4.7 %copy-start = (bf16[256,2048]{1,0:T(8,128)(2,1)S(1)}, bf16[256,2048]{1,0:T(8,128)(2,1)}, u32[]{:S(2)}) copy-start(bf16[256,2048]{1,0:T(8,128)(2,1)} %param.14) | copy-start | bytes 3145732
  6.5 5.0 %copy-start.1 = (bf16[512,128]{1,0:T(8,128)(2,1)S(1)}, bf16[512,128]{1,0:T(8,128)(2,1)}, u32[]{:S(2)}) copy-start(bf16[512,128]{1,0:T(8,128)(2,1)} %param.17) | copy-start | bytes 393220
  6.5 28.1 %copy-start.2 = (bf16[512,128]{1,0:T(8,128)(2,1)S(1)}, bf16[512,128]{1,0:T(8,128)(2,1)}, u32[]{:S(2)}) copy-start(bf16[512,128]{1,0:T(8,128)(2,1)} %param.18) | copy-start | bytes 393220
  6.5 64.6 %all-gather.7.cloned.1.call-start = ((), (), s32[]{:S(2)}) async-start(), calls=%async_computation.2 | async-start | bytes 2621440 | tf_op jit(solution)/shard_map/all_gather | solution.py:84
  7.3 111.1 %all-gather.9.cloned.1.call-start = ((), (), s32[]{:S(2)}) async-start(), calls=%async_computation.3 | async-start | bytes 2621440 | tf_op jit(solution)/shard_map/all_gather | solution.py:85
  8.0 48.4 %copy-start.7 = (f32[2048]{0:T(1024)S(1)}, f32[2048]{0:T(1024)}, u32[]{:S(2)}) copy-start(f32[2048]{0:T(1024)} %param.15) | copy-start | bytes 24580
  8.0 156.6 %all-gather.5.cloned.1.call-start = ((), (), s32[]{:S(2)}) async-start(), calls=%async_computation.1 | async-start | bytes 2621440 | tf_op jit(solution)/shard_map/all_gather | solution.py:81
  8.8 236.7 %all-gather.11.cloned.1.call-start = ((), (), s32[]{:S(2)}) async-start(), calls=%async_computation.4 | async-start | bytes 5242880 | tf_op jit(solution)/shard_map/all_gather | solution.py:156
  11.1 49.1 %copy-start.3 = (f32[31,512]{1,0:T(8,128)S(1)}, f32[31,512]{1,0:T(8,128)}, u32[]{:S(2)}) copy-start(f32[31,512]{1,0:T(8,128)} %param.22) | copy-start | bytes 190468
  11.1 49.5 %copy-start.8 = (f32[8]{0:T(128)S(1)}, f32[8]{0:T(128)}, u32[]{:S(2)}) copy-start(f32[8]{0:T(128)} %param.21) | copy-start | bytes 100
  11.2 245.8 %reduce-scatter.2.cloned.1.call-start = ((), (), s32[]{:S(2)}) async-start(), calls=%async_computation.5 | async-start | bytes 1572864 | tf_op jit(solution)/shard_map/reduce_scatter | solution.py:157
  57.4 4.8 %collective-permute-start = (bf16[128,256]{0,1:T(8,128)(2,1)S(1)}, bf16[128,256]{0,1:T(8,128)(2,1)S(1)}, u32[]{:S(2)}, u32[]{:S(2)}) collective-permute-start(bf16[128,256]{0,1:T(8,128)(2,1)S(1)} %get-tuple-element.21), channel_id=1, source_target_pairs={{0,8},{8,16},{16,24},{1,9},{9,17},{17,25},{2,10},{10,18},{18,26},{... | collective-permute-start | bytes 196616 | tf_op jit(solution)/shard_map/ppermute | solution.py:19
  58.9 10.3 %collective-permute-start.1 = (bf16[128,256]{0,1:T(8,128)(2,1)S(1)}, bf16[128,256]{0,1:T(8,128)(2,1)S(1)}, u32[]{:S(2)}, u32[]{:S(2)}) collective-permute-start(bf16[128,256]{0,1:T(8,128)(2,1)S(1)} %get-tuple-element.22), channel_id=1, source_target_pairs={{8,0},{16,8},{24,16},{9,1},{17,9},{25,17},{10,2},{18,10},{26,18},{... | collective-permute-start | bytes 196616 | tf_op jit(solution)/shard_map/ppermute | solution.py:22
  122.1 48.6 %collective-permute-start.2 = (bf16[15,512]{1,0:T(8,128)(2,1)S(1)}, bf16[15,512]{1,0:T(8,128)(2,1)S(1)}, u32[]{:S(2)}, u32[]{:S(2)}) collective-permute-start(bf16[15,512]{1,0:T(8,128)(2,1)S(1)} %get-tuple-element.15), channel_id=1, source_target_pairs={{0,8},{8,16},{16,24},{1,9},{9,17},{17,25},{2,10},{10,18},{18,26},{... | collective-permute-start | bytes 46088 | tf_op jit(solution)/shard_map/ppermute | solution.py:19
  124.2 46.5 %collective-permute-start.3 = (bf16[15,512]{1,0:T(8,128)(2,1)S(1)}, bf16[15,512]{1,0:T(8,128)(2,1)S(1)}, u32[]{:S(2)}, u32[]{:S(2)}) collective-permute-start(bf16[15,512]{1,0:T(8,128)(2,1)S(1)} %get-tuple-element.16), channel_id=1, source_target_pairs={{8,0},{16,8},{24,16},{9,1},{17,9},{25,17},{10,2},{18,10},{26,18},{... | collective-permute-start | bytes 46088 | tf_op jit(solution)/shard_map/ppermute | solution.py:22
  169.2 1.4 copy-start.4
  169.2 9.7 %copy-start.5 = (f32[512]{0:T(512)S(1)}, f32[512]{0:T(512)}, u32[]{:S(2)}) copy-start(f32[512]{0:T(512)} %param.25) | copy-start | bytes 6148
  169.2 9.7 %copy-start.6 = (f32[512]{0:T(512)S(1)}, f32[512]{0:T(512)}, u32[]{:S(2)}) copy-start(f32[512]{0:T(512)} %param.24) | copy-start | bytes 6148
Sparse Core Ops, SparseCore 0:
  8.9 62.1 all-gather.6
  72.7 45.6 all-gather.8
  120.0 44.6 all-gather.4
  166.1 79.3 all-gather.10
  250.1 6.8 reduce-scatter.1
where the time goes:
time: 264 us
  waiting for transfers between devices  172 us (65%)
  blocking collectives  49.7 us (19%)
  between operations  13.5 us (5%)
  matrix products  13.3 us (5%)
  other arithmetic  6.78 us (3%)
  starting transfers between devices  6.35 us (2%)
    all_gather x1, waiting for transfers between devices, local(): own_whole = lax.all_gather(own_rows, 'sp', axis=1, tiled=True)  66.3 us
    all_gather x1, waiting for transfers between devices, local(): piece_gate = lax.all_gather(w_conv_gate, 'sp', axis=0, tiled=True)  47.3 us
    all_gather x1, waiting for transfers between devices, local(): piece_query = lax.all_gather(w_query, 'sp', axis=0, tiled=True)  39.2 us
    all_gather x1, blocking collectives, local(): piece_key = lax.all_gather(w_key, 'sp', axis=0, tiled=True)  23.1 us
    all_gather x1, blocking collectives, local(): piece_value = lax.all_gather(w_value, 'sp', axis=0, tiled=True)  21.7 us
    reduce_scatter x1, waiting for transfers between devices, local(): lax.psum_scatter(jnp.dot(features, own_whole, preferred_element_type=jnp....  7.04 us
    ppermute x2, waiting for transfers between devices, padded(): lax.ppermute(lax.slice_in_dim(block, 0, width, axis=dim), axis, backward)  6.99 us
  transfers between devices with their start and end apart: 9, of which 7 were waited for; matrix products, arithmetic and copies ran while one was open for 7% of the time, Pallas kernels for 0%

commit v1 on v0

--- a/solution.py
+++ b/solution.py
@@ -79,8 +79,11 @@
     kv_cols = w_key.shape[1]
     chan_cols = w_conv_in.shape[1]
     piece_query = lax.all_gather(w_query, "sp", axis=0, tiled=True)
-    piece_key = lax.all_gather(w_key, "sp", axis=0, tiled=True)
-    piece_value = lax.all_gather(w_value, "sp", axis=0, tiled=True)
+    piece_key, piece_value = jnp.split(
+        lax.all_gather(jnp.concatenate([w_key, w_value], axis=1), "sp", axis=0, tiled=True),
+        [w_key.shape[1]],
+        axis=1,
+    )
     piece_conv = lax.all_gather(w_conv_in, "sp", axis=0, tiled=True)
     piece_gate = lax.all_gather(w_conv_gate, "sp", axis=0, tiled=True)
     query_acc = jnp.dot(normed, piece_query, preferred_element_type=jnp.float32)

time: 264 us -> 278 us (1.053)
  waiting for transfers between devices: 172 us -> 226 us
  blocking collectives: 49.7 us -> 4.94 us
    all_gather x2 -> x0, blocking collectives: 44.8 us -> none  [the longest x1 23.1 us: local(): piece_key = lax.all_gather(w_key, 'sp', axis=0, tiled=True)]
    all_gather x1, waiting for transfers between devices: 1.88 us -> 34.9 us  [local(): piece_conv = lax.all_gather(w_conv_in, 'sp', axis=0, tiled=True)]
    all_gather x0 -> x1, waiting for transfers between devices: none -> 25.8 us  [local(): lax.all_gather(jnp.concatenate([w_key, w_value], axis=1), 'sp', axis=0, t...]
  transfers between devices with their start and end apart: 9 -> 10, of which waited for: 7 -> 8; matrix products, arithmetic and copies ran while one was open for 7% -> 7% of each run, Pallas kernels for 0% -> 0%
where the time goes in v1:
time: 278 us
  waiting for transfers between devices  226 us (81%)
  matrix products  14.6 us (5%)
  between operations  13.8 us (5%)
  other arithmetic  8.59 us (3%)
  starting transfers between devices  8.19 us (3%)
  blocking collectives  4.94 us (2%)
    all_gather x1, waiting for transfers between devices, local(): own_whole = lax.all_gather(own_rows, 'sp', axis=1, tiled=True)  65.8 us
    all_gather x1, waiting for transfers between devices, local(): piece_gate = lax.all_gather(w_conv_gate, 'sp', axis=0, tiled=True)  46.1 us
    all_gather x1, waiting for transfers between devices, local(): piece_query = lax.all_gather(w_query, 'sp', axis=0, tiled=True)  39.5 us
    all_gather x1, waiting for transfers between devices, local(): piece_conv = lax.all_gather(w_conv_in, 'sp', axis=0, tiled=True)  34.9 us
    all_gather x1, waiting for transfers between devices, local(): lax.all_gather(jnp.concatenate([w_key, w_value], axis=1), 'sp', axis=0, t...  25.8 us
    reduce_scatter x1, waiting for transfers between devices, local(): lax.psum_scatter(jnp.dot(features, own_whole, preferred_element_type=jnp....  7.04 us
  transfers between devices with their start and end apart: 10, of which 8 were waited for; matrix products, arithmetic and copies ran while one was open for 7% of the time, Pallas kernels for 0%

profile of v1, /device:TPU:0, one launch (start us, length us, event | category | flops | bytes accessed | tf_op | source)
XLA Modules:
  0.0 277.6 jit_solution(8240120690541239744)
XLA Ops:
  6.5 0.0 copy-start
  6.5 0.0 all-gather.6.cloned.1.call-start
  6.5 1.8 pad_maximum_fusion.3
  8.3 0.0 copy-start.1
  8.3 0.0 copy-start.5
  8.3 0.0 all-gather.6.cloned.1.call-update
  8.4 0.0 all-gather.10.cloned.1.call-start
  8.4 0.7 all-gather.10.cloned.1.call-update
  9.1 0.0 all-gather.12.cloned.1.call-start
  9.2 0.7 all-gather.12.cloned.1.call-update
  9.8 0.0 all-gather.8.cloned.1.call-start
  9.9 0.5 all-gather.8.cloned.1.call-update
  10.4 0.0 all-gather.14.cloned.1.call-start
  10.5 1.3 constant_dynamic-slice_fusion
  11.7 0.0 copy-start.6
  11.8 1.1 pad_maximum_fusion
  12.8 0.0 all-gather.14.cloned.1.call-update
  12.8 0.0 reduce-scatter.2.cloned.1.call-start
  13.0 0.0 copy-done
  13.0 0.3 fusion.6
  13.3 0.0 copy-done.1
  13.3 0.2 multiply_cosine_fusion.1
  13.5 0.3 fusion.20
  13.8 25.8 %all-gather.6.cloned.1.call-done = bf16[2048,256]{1,0:T(8,128)(2,1)} async-done(((bf16[512,256]{1,0:T(8,128)(2,1)}), bf16[2048,256]{1,0:T(8,128)(2,1)}) %all-gather.6.cloned.1.call-update) | async-done | bytes 1048592 | tf_op jit(solution)/shard_map/all_gather | solution.py:83
  39.6 0.0 copy-done.5
  39.6 1.9 fusion.71
  41.7 3.4 %collective-permute-start = (bf16[128,256]{0,1:T(8,128)(2,1)S(1)}, bf16[128,256]{0,1:T(8,128)(2,1)S(1)}, u32[]{:S(2)}, u32[]{:S(2)}) collective-permute-start(bf16[128,256]{0,1:T(8,128)(2,1)S(1)} %get-tuple-element.21), channel_id=1, source_target_pairs={{0,8},{8,16},{16,24},{1,9},{9,17},{17,25},{2,10},{10,18},{18,26},{... | collective-permute-start | bytes 196616 | tf_op jit(solution)/shard_map/ppermute | solution.py:19
  45.0 1.3 collective-permute-start.1
  46.3 0.0 copy-done.6
  46.4 0.1 max.18
  46.4 0.5 collective-permute-done
  46.9 4.5 %collective-permute-done.1 = bf16[128,256]{0,1:T(8,128)(2,1)S(1)} collective-permute-done((bf16[128,256]{0,1:T(8,128)(2,1)S(1)}, bf16[128,256]{0,1:T(8,128)(2,1)S(1)}, u32[]{:S(2)}, u32[]{:S(2)}) %collective-permute-start.1) | collective-permute-done | bytes 65568 | tf_op jit(solution)/shard_map/ppermute | solution.py:22
  51.4 34.9 %all-gather.10.cloned.1.call-done = bf16[2048,512]{1,0:T(8,128)(2,1)} async-done(((bf16[512,512]{1,0:T(8,128)(2,1)}), bf16[2048,512]{1,0:T(8,128)(2,1)}) %all-gather.10.cloned.1.call-update) | async-done | bytes 2097168 | tf_op jit(solution)/shard_map/all_gather | solution.py:87
  86.3 46.1 %all-gather.12.cloned.1.call-done = bf16[2048,512]{1,0:T(8,128)(2,1)} async-done(((bf16[512,512]{1,0:T(8,128)(2,1)}), bf16[2048,512]{1,0:T(8,128)(2,1)}) %all-gather.12.cloned.1.call-update) | async-done | bytes 2097168 | tf_op jit(solution)/shard_map/all_gather | solution.py:88
  132.3 3.5 %fusion = f32[256,1024]{1,0:T(8,128)S(1)} fusion(bf16[2048,512]{1,0:T(8,128)(2,1)} %all-gather.12.cloned.1.call-done, bf16[2048,512]{1,0:T(8,128)(2,1)} %all-gather.10.cloned.1.call-done, bf16[256,2048]{1,0:T(8,128)(2,1)S(1)} %copy-done, f32[2048]{0:T(1024)S(1)} %copy-done.5, f32[256]{0:T(256)S(1)} %add_rsqrt_fusion.1), kind=kOutput, calls=%fused_computation | convolution fusion | flops 1084227584 | bytes 6300672 | tf_op jit(solution)/shard_map/dot_general | solution.py:95
  135.9 0.1 fusion.18
  136.1 2.1 collective-permute-start.2
  138.1 1.3 collective-permute-start.3
  139.4 39.5 %all-gather.8.cloned.1.call-done = bf16[2048,512]{1,0:T(8,128)(2,1)} async-done(((bf16[512,512]{1,0:T(8,128)(2,1)}), bf16[2048,512]{1,0:T(8,128)(2,1)}) %all-gather.8.cloned.1.call-update) | async-done | bytes 2097168 | tf_op jit(solution)/shard_map/all_gather | solution.py:81
  178.9 2.6 fusion.69
  181.5 0.1 subtract_convert_fusion.1
  181.6 0.8 fusion.5
  182.4 0.1 broadcast_maximum_fusion
  182.5 0.9 fusion.4
  183.4 0.1 exponential_add_fusion
  183.5 0.0 copy-start.2
  183.5 0.0 copy-start.3
  183.5 0.0 copy-start.4
  183.5 1.2 fusion.10
  184.8 0.1 copy.27
  184.9 0.0 collective-permute-done.2
  184.9 0.0 collective-permute-done.3
  184.9 0.0 copy-done.2
  184.9 3.1 %fusion.73 = (f32[256]{0:T(256)S(1)}, f32[256,512]{1,0:T(8,128)S(1)}) fusion(bf16[15,512]{1,0:T(8,128)(2,1)S(1)} %collective-permute-done.3, bf16[256,512]{1,0:T(8,128)(2,1)S(1)} %fusion.18, f32[512]{0:T(512)S(1)} %bitcast.107, f32[512]{0:T(512)S(1)} %bitcast.108, f32[512]{0:T(512)S(1)} %bitcast.79, f32[512]{0:T(512)S(1)} %bitcast.80, f32[512]{0:T(512)S(1)} %bitcast.81, ...), kind=kLoop, calls=%fused_computation.164 | loop fusion | flops 24116992 | bytes 883712 | tf_op jit(solution)/shard_map/reduce_sum | solution.py:144
  188.0 2.5 psum.14
  190.5 0.2 multiply_reduce_fusion
  190.7 2.5 psum.15
  193.2 0.0 copy-done.3
  193.2 0.0 copy-done.4
  193.2 0.3 multiply_convert_fusion
  193.5 65.8 %all-gather.14.cloned.1.call-done = bf16[1024,2048]{1,0:T(8,128)(2,1)} async-done(((bf16[1024,512]{1,0:T(8,128)(2,1)}), bf16[1024,2048]{1,0:T(8,128)(2,1)}) %all-gather.14.cloned.1.call-update) | async-done | bytes 4194320 | tf_op jit(solution)/shard_map/all_gather | solution.py:159
  259.3 4.4 %convolution_convert_fusion = bf16[256,2048]{1,0:T(8,128)(2,1)} fusion(bf16[1024,2048]{1,0:T(8,128)(2,1)} %all-gather.14.cloned.1.call-done, bf16[256,512]{1,0:T(8,128)(2,1)S(1)} %multiply_convert_fusion, bf16[256,512]{1,0:T(8,128)(2,1)S(1)} %copy.27), kind=kOutput, calls=%fused_computation.11 | convolution fusion | flops 1075314688 | bytes 5767168 | tf_op jit(solution)/shard_map/dot_general | solution.py:161
  263.7 0.0 reduce-scatter.2.cloned.1.call-update
  263.7 7.0 %reduce-scatter.2.cloned.1.call-done = bf16[128,2048]{1,0:T(8,128)(2,1)} async-done(((bf16[256,2048]{1,0:T(8,128)(2,1)}), bf16[128,2048]{1,0:T(8,128)(2,1)}) %reduce-scatter.2.cloned.1.call-update) | async-done | bytes 524304 | tf_op jit(solution)/shard_map/reduce_scatter | solution.py:160
  (18 shorter events, 0.2 us)
Async XLA Ops:
  6.5 6.4 %copy-start = (bf16[256,2048]{1,0:T(8,128)(2,1)S(1)}, bf16[256,2048]{1,0:T(8,128)(2,1)}, u32[]{:S(2)}) copy-start(bf16[256,2048]{1,0:T(8,128)(2,1)} %param.14) | copy-start | bytes 3145732
  6.5 33.1 %all-gather.6.cloned.1.call-start = ((), (), s32[]{:S(2)}) async-start(), calls=%async_computation.1 | async-start | bytes 1310720 | tf_op jit(solution)/shard_map/all_gather | solution.py:83
  8.3 5.0 %copy-start.1 = (f32[31,512]{1,0:T(8,128)S(1)}, f32[31,512]{1,0:T(8,128)}, u32[]{:S(2)}) copy-start(f32[31,512]{1,0:T(8,128)} %param.22) | copy-start | bytes 190468
  8.3 31.3 %copy-start.5 = (f32[2048]{0:T(1024)S(1)}, f32[2048]{0:T(1024)}, u32[]{:S(2)}) copy-start(f32[2048]{0:T(1024)} %param.15) | copy-start | bytes 24580
  8.4 77.9 %all-gather.10.cloned.1.call-start = ((), (), s32[]{:S(2)}) async-start(), calls=%async_computation.3 | async-start | bytes 2621440 | tf_op jit(solution)/shard_map/all_gather | solution.py:87
  9.1 123.2 %all-gather.12.cloned.1.call-start = ((), (), s32[]{:S(2)}) async-start(), calls=%async_computation.4 | async-start | bytes 2621440 | tf_op jit(solution)/shard_map/all_gather | solution.py:88
  9.8 169.0 %all-gather.8.cloned.1.call-start = ((), (), s32[]{:S(2)}) async-start(), calls=%async_computation.2 | async-start | bytes 2621440 | tf_op jit(solution)/shard_map/all_gather | solution.py:81
  10.4 248.8 %all-gather.14.cloned.1.call-start = ((), (), s32[]{:S(2)}) async-start(), calls=%async_computation.5 | async-start | bytes 5242880 | tf_op jit(solution)/shard_map/all_gather | solution.py:159
  11.7 34.6 %copy-start.6 = (f32[8]{0:T(128)S(1)}, f32[8]{0:T(128)}, u32[]{:S(2)}) copy-start(f32[8]{0:T(128)} %param.21) | copy-start | bytes 100
  12.8 257.9 %reduce-scatter.2.cloned.1.call-start = ((), (), s32[]{:S(2)}) async-start(), calls=%async_computation.6 | async-start | bytes 1572864 | tf_op jit(solution)/shard_map/reduce_scatter | solution.py:160
  41.7 5.2 %collective-permute-start = (bf16[128,256]{0,1:T(8,128)(2,1)S(1)}, bf16[128,256]{0,1:T(8,128)(2,1)S(1)}, u32[]{:S(2)}, u32[]{:S(2)}) collective-permute-start(bf16[128,256]{0,1:T(8,128)(2,1)S(1)} %get-tuple-element.21), channel_id=1, source_target_pairs={{0,8},{8,16},{16,24},{1,9},{9,17},{17,25},{2,10},{10,18},{18,26},{... | collective-permute-start | bytes 196616 | tf_op jit(solution)/shard_map/ppermute | solution.py:19
  45.0 6.3 %collective-permute-start.1 = (bf16[128,256]{0,1:T(8,128)(2,1)S(1)}, bf16[128,256]{0,1:T(8,128)(2,1)S(1)}, u32[]{:S(2)}, u32[]{:S(2)}) collective-permute-start(bf16[128,256]{0,1:T(8,128)(2,1)S(1)} %get-tuple-element.22), channel_id=1, source_target_pairs={{8,0},{16,8},{24,16},{9,1},{17,9},{25,17},{10,2},{18,10},{26,18},{... | collective-permute-start | bytes 196616 | tf_op jit(solution)/shard_map/ppermute | solution.py:22
  136.1 48.8 %collective-permute-start.2 = (bf16[15,512]{1,0:T(8,128)(2,1)S(1)}, bf16[15,512]{1,0:T(8,128)(2,1)S(1)}, u32[]{:S(2)}, u32[]{:S(2)}) collective-permute-start(bf16[15,512]{1,0:T(8,128)(2,1)S(1)} %get-tuple-element.15), channel_id=1, source_target_pairs={{0,8},{8,16},{16,24},{1,9},{9,17},{17,25},{2,10},{10,18},{18,26},{... | collective-permute-start | bytes 46088 | tf_op jit(solution)/shard_map/ppermute | solution.py:19
  138.1 46.8 %collective-permute-start.3 = (bf16[15,512]{1,0:T(8,128)(2,1)S(1)}, bf16[15,512]{1,0:T(8,128)(2,1)S(1)}, u32[]{:S(2)}, u32[]{:S(2)}) collective-permute-start(bf16[15,512]{1,0:T(8,128)(2,1)S(1)} %get-tuple-element.16), channel_id=1, source_target_pairs={{8,0},{16,8},{24,16},{9,1},{17,9},{25,17},{10,2},{18,10},{26,18},{... | collective-permute-start | bytes 46088 | tf_op jit(solution)/shard_map/ppermute | solution.py:22
  183.5 1.4 copy-start.2
  183.5 9.7 %copy-start.3 = (f32[512]{0:T(512)S(1)}, f32[512]{0:T(512)}, u32[]{:S(2)}) copy-start(f32[512]{0:T(512)} %param.25) | copy-start | bytes 6148
  183.5 9.7 %copy-start.4 = (f32[512]{0:T(512)S(1)}, f32[512]{0:T(512)}, u32[]{:S(2)}) copy-start(f32[512]{0:T(512)} %param.24) | copy-start | bytes 6148
Sparse Core Ops, SparseCore 0:
  8.9 30.6 all-gather.5
  41.2 45.0 all-gather.9
  87.8 44.4 all-gather.11
  133.8 45.0 all-gather.7
  180.3 78.9 all-gather.13
  263.8 6.8 reduce-scatter.1
